TPU v7x, 256 devices: a 4x2x16 block of a 4x16x16 slice. The times are simulated.
256 devices in a mesh: grp: 2 (over y), sp: 16 (over z), tp: 8 (over x, core).
Axes of the slice: x: 4, y: 2, z: 16, core: 2. Of those that a mesh axis runs over, the one named last changes fastest.
The devices are a block of a 4x16x16 slice.
Arguments:
- tokens: bfloat16 [32768, 2048], P(('grp', 'sp')), parts along dimension 0, may hold values from -6 to 6
- doc_ids: int32 [32768], P(('grp', 'sp')), parts along dimension 0, may hold values from 0 to 3, never falling along the last dimension, each value on 1 to 8192 neighbouring positions
- gains: bfloat16 [2, 2048], replicated, may hold values from 0.099609375 to 1.8984375
- w_query: bfloat16 [2, 2048, 1024], P(None, None, 'tp'), may hold values from -0.125 to 0.125
- w_key: bfloat16 [2, 2048, 1024], P(None, None, 'tp'), may hold values from -0.125 to 0.125
- w_value: bfloat16 [2, 2048, 1024], P(None, None, 'tp'), may hold values from -0.125 to 0.125
- rel_table: float32 [2, 16, 257], P(None, 'tp'), may hold values from -6 to 270
- out_first: bfloat16 [1024, 2048], replicated, may hold values from -0.5 to 0.5
- out_last: bfloat16 [1024, 2048], P(None, 'tp'), may hold values from -0.5 to 0.5
Outputs:
- mixed: bfloat16 [32768, 2048], P(('grp', 'sp'), 'tp'), parts along dimension 0
There are 2 independent parts, one for each index of `grp`. A program takes and returns all parts, laid end to end along the dimension named above; an argument that names none is the same for every part. Nothing has to cross between parts.
Inputs may be any that keep to these rules, and one draw needn't show every extreme that they name: `doc_ids`: document numbers never fall along the sequence.
All inputs are finite; a program needn't handle non-finite values.
Results may differ from a plain program's by a relative error of at most 0.014.
Values may be sent and summed in bfloat16 or wider, within the bound.
A program may use at most 128 MiB of HBM per device.

v0:
```python
import functools
import math

import jax
import jax.numpy as jnp
from jax import lax
from jax.experimental import pallas as pl
from jax.experimental.pallas import tpu as pltpu
from jax.sharding import PartitionSpec as P

SEG = 64
PREV_SEGS = 8
MAX_REL = 128
LAYERS = 2
HEAD_DIM = 64
REACH = SEG * PREV_SEGS
PAIR = 2 * SEG
WIN = REACH + PAIR
CHUNK = 2 * PAIR
BIG = 1e30
LOG2E = math.log2(math.e)
MESH = pl.DeviceIdType.MESH
BF = jnp.bfloat16
F32 = jnp.float32


def kernel(
    sp_n,
    tp_n,
    tokens,
    docs,
    gains,
    w_query,
    w_key,
    w_value,
    table,
    out_first,
    out_last,
    mixed,
    h,
    lhs,
    wqkv,
    wfirst,
    wlast,
    qbuf,
    qext,
    kbuf,
    kext,
    vt,
    att,
    bias,
    halo_docs,
    res,
    load_sem,
    store_sem,
    halo_send,
    halo_recv,
    ag_send,
    ag_recv,
):
    rows, width = h.shape
    cols = wlast.shape[1]
    pairs = rows // PAIR
    chunks = rows // CHUNK
    tail = REACH // CHUNK
    sp = lax.axis_index("sp")
    me = lax.axis_index("tp")
    succ = {"sp": lax.rem(sp + 1, sp_n)}
    pred = {"sp": lax.rem(sp + sp_n - 1, sp_n)}
    left_i = lax.rem(me + tp_n - 2, tp_n)
    right_i = lax.rem(me + 2, tp_n)
    far_i = lax.rem(me + 4, tp_n)
    partner_i = me + 1 - 2 * lax.rem(me, 2)
    left, right, partner = {"tp": left_i}, {"tp": right_i}, {"tp": partner_i}
    order = list(range(chunks))[::-1]

    barrier = pltpu.get_barrier_semaphore()
    for other in (left, right, partner, succ, pred):
        pl.semaphore_signal(barrier, inc=1, device_id=other, device_id_type=MESH)

    loads = {}

    def load(name, src, dst):
        copy = pltpu.make_async_copy(src, dst, load_sem.at[len(loads)])
        copy.start()
        loads[name] = copy

    def load_w(layer):
        for i, w in enumerate((w_query, w_key, w_value)):
            load(("w", layer, i), w.at[layer], wqkv.at[layer, :, pl.ds(i * 128, 128)])

    def chunk_rows(c):
        return pl.ds(c * CHUNK, CHUNK)

    load(("t", order[0]), tokens.at[chunk_rows(order[0])], h.at[chunk_rows(order[0])])
    load_w(0)
    for c in order[1:]:
        load(("t", c), tokens.at[chunk_rows(c)], h.at[chunk_rows(c)])
    load("first", out_first, wfirst)
    load_w(1)
    load("last", out_last, wlast)

    lane = lax.broadcasted_iota(jnp.int32, (PAIR, 128), 1)
    lane_f = lane.astype(F32)

    def doc_columns(row):
        return jnp.broadcast_to(row.astype(F32), (128, 128)).T

    def build_docs():
        for b in range(rows // 128):
            col = doc_columns(docs[b : b + 1, :])
            same = col == lane_f
            kext[pl.ds(REACH + 128 * b, 128), :] = jnp.where(same, 1.0, 0.0).astype(BF)
            qext[pl.ds(128 * b, 128), :] = jnp.where(same, 0.0, -BIG).astype(BF)

    def build_halo_docs():
        void = jnp.where(sp == 0, 1.0, 0.0).astype(F32)
        for b in range(REACH // 128):
            r = (rows - REACH) // 128 + b
            col = doc_columns(halo_docs[r : r + 1, :])
            one_hot = jnp.where(col == lane_f, 1.0, 0.0)
            kext[pl.ds(128 * b, 128), :] = jnp.where(lane == 127, void, one_hot).astype(BF)

    def build_bias(layer):
        row = lax.broadcasted_iota(jnp.int32, (PAIR, PAIR), 0)
        col = lax.broadcasted_iota(jnp.int32, (PAIR, PAIR), 1)
        for n in range(2):
            near = table[layer, n : n + 1, 0 : 2 * MAX_REL]
            edge = table[layer, n : n + 1, 2 * MAX_REL : 2 * MAX_REL + 1]
            near = (near - edge) * LOG2E
            upper = jnp.concatenate([near[:, 128:], jnp.zeros((1, 128), F32)], axis=1)
            for part, values in ((0, upper), (1, near)):
                turned = pltpu.roll(
                    jnp.broadcast_to(values, (128, 256)), 128, 1, stride=1, stride_axis=0
                )[:, :128]
                if part == 1:
                    turned = jnp.where((row >= SEG) & (col < SEG), -BIG, turned)
                bias[layer, pl.ds(128 * part, 128), pl.ds(128 * n, 128)] = turned

    def project_qkv(layer, c, square_sum):
        scale = lax.rsqrt(square_sum * (1.0 / width) + 1e-06)
        qkv = jnp.dot(lhs[...], wqkv[layer], preferred_element_type=F32)
        q = qkv[:, 0:128] * (scale * (HEAD_DIM**-0.5 * LOG2E))
        k = qkv[:, 128:256] * scale
        v = qkv[:, 256:384] * scale
        wide = lax.broadcasted_iota(jnp.int32, (CHUNK, 128), 1)
        qbuf[0, chunk_rows(c), :] = jnp.where(wide < HEAD_DIM, q, 0.0).astype(BF)
        qbuf[1, chunk_rows(c), :] = jnp.where(wide < HEAD_DIM, 0.0, q).astype(BF)
        kbuf[layer, pl.ds(REACH + CHUNK * c, CHUNK), :] = k.astype(BF)
        for i in range(2):
            block = v[128 * i : 128 * (i + 1), :].T
            vt[layer, REACH // 128 + 2 * c + i] = block.astype(BF)

    def gain_row(layer, n, step):
        return gains[layer : layer + 1, pl.ds(n * step, step)].astype(F32)

    def dense(c):
        step = 256
        total = jnp.zeros((CHUNK, 128), F32)
        for n in range(width // step):
            x = h[chunk_rows(c), pl.ds(n * step, step)].astype(F32)
            square = x * x
            for j in range(step // 128):
                total = total + square[:, 128 * j : 128 * (j + 1)]
            lhs[:, pl.ds(n * step, step)] = (x * gain_row(0, n, step)).astype(BF)
        project_qkv(0, c, jnp.sum(total, axis=1, keepdims=True))

    def attended_rows(layer, c):
        return jnp.concatenate([att[layer, t, chunk_rows(c), :] for t in range(tp_n)], axis=1)

    def trans(c):
        step = 256
        a = attended_rows(0, c)
        total = jnp.zeros((CHUNK, 128), F32)
        for n in range(width // step):
            part = pl.ds(n * step, step)
            update = jnp.dot(a, wfirst[:, part], preferred_element_type=F32)
            x = (h[chunk_rows(c), part].astype(F32) + update).astype(BF)
            h[chunk_rows(c), part] = x
            x = x.astype(F32)
            square = x * x
            for j in range(step // 128):
                total = total + square[:, 128 * j : 128 * (j + 1)]
            lhs[:, part] = (x * gain_row(1, n, step)).astype(BF)
        project_qkv(1, c, jnp.sum(total, axis=1, keepdims=True))

    def final(c):
        a = attended_rows(1, c)
        update = jnp.dot(a, wlast[...], preferred_element_type=F32)
        own = h[chunk_rows(c), pl.ds(pl.multiple_of(me * cols, cols), cols)].astype(F32)
        res[chunk_rows(c), :] = (own + update).astype(BF)
        copy = pltpu.make_async_copy(
            res.at[chunk_rows(c)], mixed.at[chunk_rows(c)], store_sem.at[c]
        )
        copy.start()
        return copy

    def attend(layer, p):
        window = pl.ds(PAIR * p, WIN)
        mine = pl.ds(PAIR * p, PAIR)
        keys = jnp.concatenate([kbuf[layer, window, :], kext[window, :]], axis=1)
        queries = jnp.concatenate(
            [
                jnp.concatenate([qbuf[0, mine, :], qext[mine, :]], axis=1),
                jnp.concatenate([qbuf[1, mine, :], qext[mine, :]], axis=1),
            ],
            axis=0,
        )
        s = lax.dot_general(
            keys, queries, (((1,), (1,)), ((), ())), preferred_element_type=F32
        )
        first = lax.broadcasted_iota(jnp.int32, (SEG, 2 * PAIR), 1)
        s_first = jnp.where(lax.rem(first, PAIR) < SEG, s[:SEG], -BIG)
        s = jnp.concatenate([s_first, s[SEG : WIN - 256], s[WIN - 256 :] + bias[layer]], axis=0)
        e = jnp.exp2(s - jnp.max(s, axis=0, keepdims=True))
        inverse = 1.0 / jnp.sum(e, axis=0, keepdims=True)
        values = jnp.concatenate([vt[layer, p + i] for i in range(WIN // 128)], axis=1)
        o = jnp.dot(values, e.astype(BF), preferred_element_type=F32)
        o = jnp.concatenate(
            [
                o[:HEAD_DIM, :PAIR] * inverse[:, :PAIR],
                o[HEAD_DIM:, PAIR:] * inverse[:, PAIR:],
            ],
            axis=0,
        )
        att[layer, me, mine, :] = o.T.astype(BF)

    sent = []

    def remote(src, dst, send_sem, recv_sem, device):
        return pltpu.make_async_remote_copy(
            src_ref=src,
            dst_ref=dst,
            send_sem=send_sem,
            recv_sem=recv_sem,
            device_id=device,
            device_id_type=MESH,
        )

    def start(copy):
        copy.start()
        sent.append(copy)

    def halo(layer, c):
        i = layer * tail + c - (chunks - tail)
        k0 = CHUNK * (c - (chunks - tail))
        b0 = k0 // 128
        return (
            remote(
                kbuf.at[layer, pl.ds(REACH + CHUNK * c, CHUNK)],
                kbuf.at[layer, pl.ds(k0, CHUNK)],
                halo_send.at[2 * i],
                halo_recv.at[2 * i],
                succ,
            ),
            remote(
                vt.at[layer, pl.ds(REACH // 128 + 2 * c, 2)],
                vt.at[layer, pl.ds(b0, 2)],
                halo_send.at[2 * i + 1],
                halo_recv.at[2 * i + 1],
                succ,
            ),
        )

    def doc_halo():
        i = 2 * LAYERS * tail
        return remote(docs, halo_docs, halo_send.at[i], halo_recv.at[i], succ)

    def send_halo(layer, c):
        for copy in halo(layer, c):
            start(copy)

    def wait_halo(layer, c):
        for copy in halo(layer, c):
            copy.wait_recv()

    def block(layer, p, kind, slot, device, part=None):
        first = PAIR * p + (SEG if part == 1 else 0)
        ref = att.at[layer, slot, pl.ds(first, PAIR if part is None else SEG)]
        i = (layer * pairs + p) * 8 + kind
        return remote(ref, ref, ag_send.at[i], ag_recv.at[i], device)

    def send_own(layer, p):
        start(block(layer, p, 0, me, right))
        start(block(layer, p, 1, me, left))
        start(block(layer, p, 2, me, partner))

    def relay1(layer, p):
        block(layer, p, 0, left_i, right).wait_recv()
        start(block(layer, p, 3, left_i, right, 0))
        start(block(layer, p, 4, left_i, partner))
        block(layer, p, 1, right_i, left).wait_recv()
        start(block(layer, p, 5, right_i, left, 1))
        start(block(layer, p, 6, right_i, partner))

    def relay2(layer, p):
        block(layer, p, 3, far_i, right, 0).wait_recv()
        block(layer, p, 5, far_i, left, 1).wait_recv()
        start(block(layer, p, 7, far_i, partner))

    def consume(layer, p):
        block(layer, p, 2, partner_i, partner).wait_recv()
        block(layer, p, 4, lax.rem(partner_i + tp_n - 2, tp_n), partner).wait_recv()
        block(layer, p, 6, lax.rem(partner_i + 2, tp_n), partner).wait_recv()
        block(layer, p, 7, lax.rem(partner_i + 4, tp_n), partner).wait_recv()

    def attend_send(layer, *which):
        for p in which:
            attend(layer, p)
            send_own(layer, p)

    build_docs()
    for layer in range(LAYERS):
        build_bias(layer)
    for i in range(3):
        loads[("w", 0, i)].wait()
    c3, c2, c1, c0 = order
    loads[("t", c3)].wait()
    dense(c3)
    pl.semaphore_wait(barrier, 5)
    start(doc_halo())
    send_halo(0, c3)
    loads[("t", c2)].wait()
    dense(c2)
    send_halo(0, c2)
    loads[("t", c1)].wait()
    dense(c1)
    attend_send(0, 7, 6)
    loads[("t", c0)].wait()
    dense(c0)
    attend_send(0, 5, 4)
    doc_halo().wait_recv()
    build_halo_docs()
    wait_halo(0, c3)
    attend_send(0, 3, 2)
    relay1(0, 7)
    relay1(0, 6)
    wait_halo(0, c2)
    attend_send(0, 1, 0)
    relay1(0, 5)
    relay2(0, 7)
    relay1(0, 4)
    relay2(0, 6)
    relay1(0, 3)
    loads["first"].wait()
    for i in range(3):
        loads[("w", 1, i)].wait()
    loads["last"].wait()
    consume(0, 7)
    consume(0, 6)
    trans(c3)
    send_halo(1, c3)
    relay2(0, 5)
    relay1(0, 2)
    relay2(0, 4)
    relay1(0, 1)
    relay1(0, 0)
    consume(0, 5)
    consume(0, 4)
    trans(c2)
    send_halo(1, c2)
    relay2(0, 3)
    relay2(0, 2)
    relay2(0, 1)
    relay2(0, 0)
    consume(0, 3)
    consume(0, 2)
    trans(c1)
    attend_send(1, 7, 6)
    consume(0, 1)
    consume(0, 0)
    trans(c0)
    relay1(1, 7)
    attend_send(1, 5, 4)
    relay1(1, 6)
    wait_halo(1, c3)
    attend_send(1, 3, 2)
    relay1(1, 5)
    relay2(1, 7)
    wait_halo(1, c2)
    attend_send(1, 1, 0)
    relay1(1, 4)
    relay2(1, 6)
    relay1(1, 3)
    relay2(1, 5)
    consume(1, 7)
    consume(1, 6)
    stores = [final(c3)]
    relay1(1, 2)
    relay2(1, 4)
    relay1(1, 1)
    relay2(1, 3)
    relay1(1, 0)
    consume(1, 5)
    consume(1, 4)
    stores.append(final(c2))
    relay2(1, 2)
    relay2(1, 1)
    relay2(1, 0)
    consume(1, 3)
    consume(1, 2)
    stores.append(final(c1))
    consume(1, 1)
    consume(1, 0)
    stores.append(final(c0))
    for copy in sent:
        copy.wait_send()
    for copy in stores:
        copy.wait()


def solution(mesh):
    sp_n, tp_n = mesh.shape["sp"], mesh.shape["tp"]

    def shards(tokens, doc_ids, gains, w_query, w_key, w_value, rel_table, out_first, out_last):
        rows, width = tokens.shape
        cols = out_last.shape[1]
        depth = out_first.shape[0]
        heads = w_query.shape[2]
        tail = REACH // CHUNK
        halos = 2 * LAYERS * tail + 1
        copies = LAYERS * (rows // PAIR) * 8
        anywhere = pl.BlockSpec(memory_space=pl.ANY)
        vmem = pl.BlockSpec(memory_space=pltpu.VMEM)
        return pl.pallas_call(
            functools.partial(kernel, sp_n, tp_n),
            out_shape=jax.ShapeDtypeStruct((rows, cols), BF),
            in_specs=[anywhere, vmem, vmem, anywhere, anywhere, anywhere, vmem, anywhere, anywhere],
            out_specs=anywhere,
            scratch_shapes=[
                pltpu.VMEM((rows, width), BF),
                pltpu.VMEM((CHUNK, width), BF),
                pltpu.VMEM((LAYERS, width, 3 * heads), BF),
                pltpu.VMEM((depth, width), BF),
                pltpu.VMEM((depth, cols), BF),
                pltpu.VMEM((2, rows, heads), BF),
                pltpu.VMEM((rows, 128), BF),
                pltpu.VMEM((LAYERS, REACH + rows, heads), BF),
                pltpu.VMEM((REACH + rows, 128), BF),
                pltpu.VMEM((LAYERS, (REACH + rows) // 128, heads, 128), BF),
                pltpu.VMEM((LAYERS, tp_n, rows, heads), BF),
                pltpu.VMEM((LAYERS, 256, 2 * PAIR), F32),
                pltpu.VMEM((rows // 128, 128), jnp.int32),
                pltpu.VMEM((rows, cols), BF),
                pltpu.SemaphoreType.DMA((3 * LAYERS + rows // CHUNK + 2,)),
                pltpu.SemaphoreType.DMA((rows // CHUNK,)),
                pltpu.SemaphoreType.DMA((halos,)),
                pltpu.SemaphoreType.DMA((halos,)),
                pltpu.SemaphoreType.DMA((copies,)),
                pltpu.SemaphoreType.DMA((copies,)),
            ],
            compiler_params=pltpu.CompilerParams(
                collective_id=0, has_side_effects=True, vmem_limit_bytes=60 * 1024 * 1024
            ),
        )(
            tokens,
            doc_ids.reshape(rows // 128, 128),
            gains,
            w_query,
            w_key,
            w_value,
            rel_table,
            out_first,
            out_last,
        )

    placed = (
        P(("grp", "sp"), None),
        P(("grp", "sp")),
        P(),
        P(None, None, "tp"),
        P(None, None, "tp"),
        P(None, None, "tp"),
        P(None, "tp", None),
        P(),
        P(None, "tp"),
    )
    return jax.shard_map(
        shards, mesh=mesh, in_specs=placed, out_specs=P(("grp", "sp"), "tp"), check_vma=False
    )
```

profile of v0, /device:TPU:33, one launch (start us, length us, event | category | flops | bytes accessed | tf_op | source)
XLA Modules:
  0.0 71.6 jit_solution(13095715376082415191)
XLA Ops:
  0.0 69.7 %shard_map.91 = bf16[1024,256]{1,0:T(8,128)(2,1)} custom-call(bf16[1024,2048]{1,0:T(8,128)(2,1)} %tokens.1, s32[8,128]{1,0:T(8,128)} %bitcast.1, bf16[2,2048]{1,0:T(2,128)(2,1)} %gains.1, bf16[2,2048,128]{2,1,0:T(8,128)(2,1)} %w_query.1, bf16[2,2048,128]{2,1,0:T(8,128)(2,1)} %w_key.1, bf16[2,2048,128]{2,1,0:T(8,128)(2,1)} %w_value.1, f32[2,2,257]{2,1,0:T(2,128)} %table.1, ...), custom_call_target="tpu_custom_call" | custom-call | tf_op jit(solution)/shard_map/pallas_call | solution.py:425
  69.7 1.9 %copy.11 = bf16[1024,256]{1,0:T(8,128)(2,1)} copy(bf16[1024,256]{1,0:T(8,128)(2,1)} %shard_map.91) | data formatting | bytes 1048576
where the time goes:
time: 71.7 us; the launch traced here: 71.6 us
  Pallas kernels  69.7 us (97%)
  local copies, waits for them, and re-layouts  1.87 us (3%)
    pallas_call x1, Pallas kernels, shards(): pl.pallas_call(functools.partial(kernel, sp_n, tp_n), out_shape=jax.Shape...  69.7 us
    unnamed x1, local copies, waits for them, and re-layouts  1.87 us

commit v1 on v0

--- a/solution.py
+++ b/solution.py
@@ -18,25 +18,38 @@
 WIN = REACH + PAIR
 CHUNK = 2 * PAIR
 BIG = 1e30
+DIRECT = (7, 6, 1, 0)
 LOG2E = math.log2(math.e)
 MESH = pl.DeviceIdType.MESH
 BF = jnp.bfloat16
 F32 = jnp.float32
 
 
+def scoped(f):
+    @functools.wraps(f)
+    def inner(*which, **named):
+        with jax.named_scope("_".join([f.__name__, *map(str, which[:4])])):
+            return f(*which, **named)
+
+    return inner
+
+
 def kernel(
     sp_n,
     tp_n,
     tokens,
-    docs,
-    gains,
+    docs_in,
+    gains_in,
     w_query,
     w_key,
     w_value,
-    table,
+    table_in,
     out_first,
     out_last,
     mixed,
+    docs,
+    gains,
+    table,
     h,
     lhs,
     wqkv,
@@ -50,13 +63,13 @@
     att,
     bias,
     halo_docs,
-    res,
     load_sem,
-    store_sem,
     halo_send,
     halo_recv,
     ag_send,
-    ag_recv,
+    near_recv,
+    far_recv,
+    partner_recv,
 ):
     rows, width = h.shape
     cols = wlast.shape[1]
@@ -71,34 +84,58 @@
     right_i = lax.rem(me + 2, tp_n)
     far_i = lax.rem(me + 4, tp_n)
     partner_i = me + 1 - 2 * lax.rem(me, 2)
-    left, right, partner = {"tp": left_i}, {"tp": right_i}, {"tp": partner_i}
+    left, right, far, partner = {"tp": left_i}, {"tp": right_i}, {"tp": far_i}, {"tp": partner_i}
     order = list(range(chunks))[::-1]
 
-    barrier = pltpu.get_barrier_semaphore()
-    for other in (left, right, partner, succ, pred):
-        pl.semaphore_signal(barrier, inc=1, device_id=other, device_id_type=MESH)
-
     loads = {}
 
-    def load(name, src, dst):
-        copy = pltpu.make_async_copy(src, dst, load_sem.at[len(loads)])
-        copy.start()
+    def load(name, *pairs_of_refs, whole=None):
+        sem = load_sem.at[len(loads)]
+        for src, dst in pairs_of_refs:
+            copy = pltpu.make_async_copy(src, dst, sem)
+            copy.start()
+        if whole is not None:
+            copy = pltpu.make_async_copy(whole, whole, sem)
         loads[name] = copy
 
     def load_w(layer):
-        for i, w in enumerate((w_query, w_key, w_value)):
-            load(("w", layer, i), w.at[layer], wqkv.at[layer, :, pl.ds(i * 128, 128)])
+        load(
+            ("w", layer),
+            *(
+                (w.at[layer], wqkv.at[layer, :, pl.ds(i * 128, 128)])
+                for i, w in enumerate((w_query, w_key, w_value))
+            ),
+            whole=wqkv.at[layer],
+        )
 
     def chunk_rows(c):
         return pl.ds(c * CHUNK, CHUNK)
 
-    load(("t", order[0]), tokens.at[chunk_rows(order[0])], h.at[chunk_rows(order[0])])
+    def load_tokens(c):
+        load(("t", c), (tokens.at[chunk_rows(c)], h.at[chunk_rows(c)]))
+
+    load("docs", (docs_in, docs))
+    load("gains", (gains_in, gains))
+    load("table", (table_in, table))
+    load_tokens(order[0])
     load_w(0)
     for c in order[1:]:
-        load(("t", c), tokens.at[chunk_rows(c)], h.at[chunk_rows(c)])
-    load("first", out_first, wfirst)
+        load_tokens(c)
+    load("first", (out_first, wfirst))
     load_w(1)
-    load("last", out_last, wlast)
+    load("last", (out_last, wlast))
+
+    barrier = pltpu.get_barrier_semaphore()
+    for other in (left, right, far, partner):
+        pl.semaphore_signal(barrier, inc=1, device_id=other, device_id_type=MESH)
+
+    @pl.when(sp < sp_n - 1)
+    def _():
+        pl.semaphore_signal(barrier, inc=1, device_id=succ, device_id_type=MESH)
+
+    @pl.when(sp > 0)
+    def _():
+        pl.semaphore_signal(barrier, inc=1, device_id=pred, device_id_type=MESH)
 
     lane = lax.broadcasted_iota(jnp.int32, (PAIR, 128), 1)
     lane_f = lane.astype(F32)
@@ -154,6 +191,7 @@
     def gain_row(layer, n, step):
         return gains[layer : layer + 1, pl.ds(n * step, step)].astype(F32)
 
+    @scoped
     def dense(c):
         step = 256
         total = jnp.zeros((CHUNK, 128), F32)
@@ -168,7 +206,8 @@
     def attended_rows(layer, c):
         return jnp.concatenate([att[layer, t, chunk_rows(c), :] for t in range(tp_n)], axis=1)
 
-    def trans(c):
+    @scoped
+    def trans(c, between=None):
         step = 256
         a = attended_rows(0, c)
         total = jnp.zeros((CHUNK, 128), F32)
@@ -182,20 +221,18 @@
             for j in range(step // 128):
                 total = total + square[:, 128 * j : 128 * (j + 1)]
             lhs[:, part] = (x * gain_row(1, n, step)).astype(BF)
+            if between is not None and n == width // step // 2 - 1:
+                between()
         project_qkv(1, c, jnp.sum(total, axis=1, keepdims=True))
 
+    @scoped
     def final(c):
         a = attended_rows(1, c)
         update = jnp.dot(a, wlast[...], preferred_element_type=F32)
         own = h[chunk_rows(c), pl.ds(pl.multiple_of(me * cols, cols), cols)].astype(F32)
-        res[chunk_rows(c), :] = (own + update).astype(BF)
-        copy = pltpu.make_async_copy(
-            res.at[chunk_rows(c)], mixed.at[chunk_rows(c)], store_sem.at[c]
-        )
-        copy.start()
-        return copy
-
-    def attend(layer, p):
+        mixed[chunk_rows(c), :] = (own + update).astype(BF)
+
+    def scores_of(layer, p):
         window = pl.ds(PAIR * p, WIN)
         mine = pl.ds(PAIR * p, PAIR)
         keys = jnp.concatenate([kbuf[layer, window, :], kext[window, :]], axis=1)
@@ -211,7 +248,11 @@
         )
         first = lax.broadcasted_iota(jnp.int32, (SEG, 2 * PAIR), 1)
         s_first = jnp.where(lax.rem(first, PAIR) < SEG, s[:SEG], -BIG)
-        s = jnp.concatenate([s_first, s[SEG : WIN - 256], s[WIN - 256 :] + bias[layer]], axis=0)
+        return jnp.concatenate(
+            [s_first, s[SEG : WIN - 256], s[WIN - 256 :] + bias[layer]], axis=0
+        )
+
+    def weigh(layer, p, s):
         e = jnp.exp2(s - jnp.max(s, axis=0, keepdims=True))
         inverse = 1.0 / jnp.sum(e, axis=0, keepdims=True)
         values = jnp.concatenate([vt[layer, p + i] for i in range(WIN // 128)], axis=1)
@@ -223,9 +264,13 @@
             ],
             axis=0,
         )
-        att[layer, me, mine, :] = o.T.astype(BF)
-
-    sent = []
+        att[layer, me, pl.ds(PAIR * p, PAIR), :] = o.T.astype(BF)
+
+    @scoped
+    def attend(layer, *which):
+        scores = [scores_of(layer, p) for p in which]
+        for p, s in zip(which, scores):
+            weigh(layer, p, s)
 
     def remote(src, dst, send_sem, recv_sem, device):
         return pltpu.make_async_remote_copy(
@@ -236,10 +281,6 @@
             device_id=device,
             device_id_type=MESH,
         )
-
-    def start(copy):
-        copy.start()
-        sent.append(copy)
 
     def halo(layer, c):
         i = layer * tail + c - (chunks - tail)
@@ -266,60 +307,105 @@
         i = 2 * LAYERS * tail
         return remote(docs, halo_docs, halo_send.at[i], halo_recv.at[i], succ)
 
+    halos = []
+
     def send_halo(layer, c):
-        for copy in halo(layer, c):
-            start(copy)
-
+        halos.extend(halo(layer, c))
+
+        @pl.when(sp < sp_n - 1)
+        def _():
+            for copy in halo(layer, c):
+                copy.start()
+
+    @scoped
     def wait_halo(layer, c):
-        for copy in halo(layer, c):
-            copy.wait_recv()
-
-    def block(layer, p, kind, slot, device, part=None):
+        @pl.when(sp > 0)
+        def _():
+            for copy in halo(layer, c):
+                copy.wait_recv()
+
+    sent = [0] * LAYERS
+
+    def send(layer, p, slot, device, recv_sem, part=None):
         first = PAIR * p + (SEG if part == 1 else 0)
-        ref = att.at[layer, slot, pl.ds(first, PAIR if part is None else SEG)]
-        i = (layer * pairs + p) * 8 + kind
-        return remote(ref, ref, ag_send.at[i], ag_recv.at[i], device)
+        count = PAIR if part is None else SEG
+        ref = att.at[layer, slot, pl.ds(first, count)]
+        remote(ref, ref, ag_send.at[layer], recv_sem, device).start()
+        sent[layer] += count
+
+    def arrived(layer, slots, count, recv_sem):
+        ref = att.at[layer, 0:slots, pl.ds(0, count)]
+        remote(ref, ref, ag_send.at[layer], recv_sem, partner).wait_recv()
+
+    def near_sem(layer, p):
+        return near_recv.at[layer * pairs + p]
+
+    def far_sem(layer, p):
+        return far_recv.at[layer * pairs + p]
+
+    def partner_sem(layer, p):
+        return partner_recv.at[layer * chunks + p // 2]
+
+    def is_direct(layer, p):
+        return layer == 0 or p in DIRECT
 
     def send_own(layer, p):
-        start(block(layer, p, 0, me, right))
-        start(block(layer, p, 1, me, left))
-        start(block(layer, p, 2, me, partner))
-
-    def relay1(layer, p):
-        block(layer, p, 0, left_i, right).wait_recv()
-        start(block(layer, p, 3, left_i, right, 0))
-        start(block(layer, p, 4, left_i, partner))
-        block(layer, p, 1, right_i, left).wait_recv()
-        start(block(layer, p, 5, right_i, left, 1))
-        start(block(layer, p, 6, right_i, partner))
-
-    def relay2(layer, p):
-        block(layer, p, 3, far_i, right, 0).wait_recv()
-        block(layer, p, 5, far_i, left, 1).wait_recv()
-        start(block(layer, p, 7, far_i, partner))
-
-    def consume(layer, p):
-        block(layer, p, 2, partner_i, partner).wait_recv()
-        block(layer, p, 4, lax.rem(partner_i + tp_n - 2, tp_n), partner).wait_recv()
-        block(layer, p, 6, lax.rem(partner_i + 2, tp_n), partner).wait_recv()
-        block(layer, p, 7, lax.rem(partner_i + 4, tp_n), partner).wait_recv()
+        send(layer, p, me, right, near_sem(layer, p))
+        send(layer, p, me, left, near_sem(layer, p))
+        if is_direct(layer, p):
+            send(layer, p, me, far, far_sem(layer, p))
+        send(layer, p, me, partner, partner_sem(layer, p))
+
+    @scoped
+    def near(layer, *which):
+        for p in which:
+            arrived(layer, 2, PAIR, near_sem(layer, p))
+            if not is_direct(layer, p):
+                send(layer, p, left_i, right, far_sem(layer, p), 0)
+                send(layer, p, right_i, left, far_sem(layer, p), 1)
+            send(layer, p, left_i, partner, partner_sem(layer, p))
+            send(layer, p, right_i, partner, partner_sem(layer, p))
+
+    @scoped
+    def distant(layer, *which):
+        for p in which:
+            arrived(layer, 1, PAIR, far_sem(layer, p))
+            send(layer, p, far_i, partner, partner_sem(layer, p))
+
+    @scoped
+    def consume(layer, c):
+        arrived(layer, tp_n, PAIR, partner_sem(layer, 2 * c))
 
     def attend_send(layer, *which):
+        attend(layer, *which)
         for p in which:
-            attend(layer, p)
             send_own(layer, p)
 
+    @pl.when(sp == 0)
+    def _():
+        for layer in range(LAYERS):
+            kbuf[layer, 0:REACH, :] = jnp.zeros((REACH, 128), BF)
+            for b in range(REACH // 128):
+                vt[layer, b] = jnp.zeros((128, 128), BF)
+        halo_docs[...] = jnp.zeros(halo_docs.shape, jnp.int32)
+
+    loads["docs"].wait()
     build_docs()
-    for layer in range(LAYERS):
-        build_bias(layer)
-    for i in range(3):
-        loads[("w", 0, i)].wait()
+    loads["table"].wait()
+    build_bias(0)
+    loads["gains"].wait()
+    loads[("w", 0)].wait()
     c3, c2, c1, c0 = order
     loads[("t", c3)].wait()
     dense(c3)
-    pl.semaphore_wait(barrier, 5)
-    start(doc_halo())
+    with jax.named_scope("barrier"):
+        pl.semaphore_wait(barrier, 4 + jnp.where(sp > 0, 1, 0) + jnp.where(sp < sp_n - 1, 1, 0))
     send_halo(0, c3)
+
+    @pl.when(sp < sp_n - 1)
+    def _():
+        doc_halo().start()
+
     loads[("t", c2)].wait()
     dense(c2)
     send_halo(0, c2)
@@ -329,84 +415,82 @@
     loads[("t", c0)].wait()
     dense(c0)
     attend_send(0, 5, 4)
-    doc_halo().wait_recv()
+
+    @pl.when(sp > 0)
+    def _():
+        doc_halo().wait_recv()
+
     build_halo_docs()
     wait_halo(0, c3)
     attend_send(0, 3, 2)
-    relay1(0, 7)
-    relay1(0, 6)
+    build_bias(1)
+    loads["first"].wait()
+    loads[("w", 1)].wait()
+    loads["last"].wait()
+    near(0, 7, 6)
     wait_halo(0, c2)
     attend_send(0, 1, 0)
-    relay1(0, 5)
-    relay2(0, 7)
-    relay1(0, 4)
-    relay2(0, 6)
-    relay1(0, 3)
-    loads["first"].wait()
-    for i in range(3):
-        loads[("w", 1, i)].wait()
-    loads["last"].wait()
-    consume(0, 7)
-    consume(0, 6)
-    trans(c3)
+    distant(0, 7, 6)
+    near(0, 5, 4)
+    consume(0, c3)
+
+    def serve_0():
+        distant(0, 5, 4)
+        near(0, 3)
+
+    def serve_1():
+        near(0, 2)
+        distant(0, 3, 2)
+
+    def serve_2():
+        near(0, 1, 0)
+        distant(0, 1, 0)
+
+    trans(c3, between=serve_0)
     send_halo(1, c3)
-    relay2(0, 5)
-    relay1(0, 2)
-    relay2(0, 4)
-    relay1(0, 1)
-    relay1(0, 0)
-    consume(0, 5)
-    consume(0, 4)
-    trans(c2)
+    consume(0, c2)
+    trans(c2, between=serve_1)
     send_halo(1, c2)
-    relay2(0, 3)
-    relay2(0, 2)
-    relay2(0, 1)
-    relay2(0, 0)
-    consume(0, 3)
-    consume(0, 2)
-    trans(c1)
+    consume(0, c1)
+    trans(c1, between=serve_2)
     attend_send(1, 7, 6)
-    consume(0, 1)
-    consume(0, 0)
+    consume(0, c0)
     trans(c0)
-    relay1(1, 7)
     attend_send(1, 5, 4)
-    relay1(1, 6)
+    near(1, 7, 6)
     wait_halo(1, c3)
     attend_send(1, 3, 2)
-    relay1(1, 5)
-    relay2(1, 7)
+    distant(1, 7, 6)
     wait_halo(1, c2)
     attend_send(1, 1, 0)
-    relay1(1, 4)
-    relay2(1, 6)
-    relay1(1, 3)
-    relay2(1, 5)
-    consume(1, 7)
-    consume(1, 6)
-    stores = [final(c3)]
-    relay1(1, 2)
-    relay2(1, 4)
-    relay1(1, 1)
-    relay2(1, 3)
-    relay1(1, 0)
-    consume(1, 5)
-    consume(1, 4)
-    stores.append(final(c2))
-    relay2(1, 2)
-    relay2(1, 1)
-    relay2(1, 0)
-    consume(1, 3)
-    consume(1, 2)
-    stores.append(final(c1))
-    consume(1, 1)
-    consume(1, 0)
-    stores.append(final(c0))
-    for copy in sent:
-        copy.wait_send()
-    for copy in stores:
-        copy.wait()
+    near(1, 5, 4)
+    consume(1, c3)
+    final(c3)
+    near(1, 3, 2)
+    distant(1, 5, 4)
+    near(1, 1, 0)
+    distant(1, 3, 2)
+    consume(1, c2)
+    final(c2)
+    consume(1, c1)
+    final(c1)
+    distant(1, 1, 0)
+    consume(1, c0)
+    final(c0)
+    with jax.named_scope("sends"):
+        for layer in range(LAYERS):
+            whole, rest = divmod(sent[layer], rows)
+            ref = att.at[layer, 0:whole]
+            remote(ref, ref, ag_send.at[layer], near_sem(layer, 0), partner).wait_send()
+            if rest:
+                ref = att.at[layer, 0, pl.ds(0, rest)]
+                remote(ref, ref, ag_send.at[layer], near_sem(layer, 0), partner).wait_send()
+
+        @pl.when(sp < sp_n - 1)
+        def _():
+            doc_halo().wait_send()
+            for copy in halos:
+                copy.wait_send()
 
 
 def solution(mesh):
@@ -419,15 +503,17 @@
         heads = w_query.shape[2]
         tail = REACH // CHUNK
         halos = 2 * LAYERS * tail + 1
-        copies = LAYERS * (rows // PAIR) * 8
-        anywhere = pl.BlockSpec(memory_space=pl.ANY)
+        anywhere = pl.BlockSpec(memory_space=pltpu.HBM)
         vmem = pl.BlockSpec(memory_space=pltpu.VMEM)
         return pl.pallas_call(
             functools.partial(kernel, sp_n, tp_n),
             out_shape=jax.ShapeDtypeStruct((rows, cols), BF),
-            in_specs=[anywhere, vmem, vmem, anywhere, anywhere, anywhere, vmem, anywhere, anywhere],
-            out_specs=anywhere,
+            in_specs=[anywhere] * 9,
+            out_specs=vmem,
             scratch_shapes=[
+                pltpu.VMEM((rows // 128, 128), jnp.int32),
+                pltpu.VMEM(gains.shape, gains.dtype),
+                pltpu.VMEM(rel_table.shape, rel_table.dtype),
                 pltpu.VMEM((rows, width), BF),
                 pltpu.VMEM((CHUNK, width), BF),
                 pltpu.VMEM((LAYERS, width, 3 * heads), BF),
@@ -441,13 +527,13 @@
                 pltpu.VMEM((LAYERS, tp_n, rows, heads), BF),
                 pltpu.VMEM((LAYERS, 256, 2 * PAIR), F32),
                 pltpu.VMEM((rows // 128, 128), jnp.int32),
-                pltpu.VMEM((rows, cols), BF),
-                pltpu.SemaphoreType.DMA((3 * LAYERS + rows // CHUNK + 2,)),
-                pltpu.SemaphoreType.DMA((rows // CHUNK,)),
+                pltpu.SemaphoreType.DMA((LAYERS + rows // CHUNK + 5,)),
                 pltpu.SemaphoreType.DMA((halos,)),
                 pltpu.SemaphoreType.DMA((halos,)),
-                pltpu.SemaphoreType.DMA((copies,)),
-                pltpu.SemaphoreType.DMA((copies,)),
+                pltpu.SemaphoreType.DMA((LAYERS,)),
+                pltpu.SemaphoreType.DMA((LAYERS * (rows // PAIR),)),
+                pltpu.SemaphoreType.DMA((LAYERS * (rows // PAIR),)),
+                pltpu.SemaphoreType.DMA((LAYERS * (rows // CHUNK),)),
             ],
             compiler_params=pltpu.CompilerParams(
                 collective_id=0, has_side_effects=True, vmem_limit_bytes=60 * 1024 * 1024

time: 71.7 us -> 61.8 us (0.86)
  Pallas kernels: 69.7 us -> 59.8 us
    pallas_call x1, Pallas kernels: 69.7 us -> 59.8 us  [shards(): pl.pallas_call(functools.partial(kernel, sp_n, tp_n), out_shape=jax.Shape...]
where the time goes in v1:
time: 61.8 us; the launch traced here: 61.6 us
  Pallas kernels  59.8 us (97%)
  local copies, waits for them, and re-layouts  1.87 us (3%)
    pallas_call x1, Pallas kernels, shards(): pl.pallas_call(functools.partial(kernel, sp_n, tp_n), out_shape=jax.Shape...  59.8 us
    unnamed x1, local copies, waits for them, and re-layouts  1.87 us

profile of v1, /device:TPU:33, one launch (start us, length us, event | category | flops | bytes accessed | tf_op | source)
XLA Modules:
  0.0 61.6 jit_solution(18154484203318497753)
XLA Ops:
  0.0 59.8 %shard_map.91 = bf16[1024,256]{1,0:T(8,128)(2,1)} custom-call(bf16[1024,2048]{1,0:T(8,128)(2,1)} %tokens.1, s32[8,128]{1,0:T(8,128)} %bitcast.1, bf16[2,2048]{1,0:T(2,128)(2,1)} %gains_in.1, bf16[2,2048,128]{2,1,0:T(8,128)(2,1)} %w_query.1, bf16[2,2048,128]{2,1,0:T(8,128)(2,1)} %w_key.1, bf16[2,2048,128]{2,1,0:T(8,128)(2,1)} %w_value.1, ...), custom_call_target="tpu_custom_call" | custom-call | tf_op jit(solution)/shard_map/pallas_call | solution.py:508
  59.8 1.9 %copy.11 = bf16[1024,256]{1,0:T(8,128)(2,1)} copy(bf16[1024,256]{1,0:T(8,128)(2,1)} %shard_map.91) | data formatting | bytes 1048576

commit v2 on v1

--- a/solution.py
+++ b/solution.py
@@ -121,10 +121,6 @@
     load_w(0)
     for c in order[1:]:
         load_tokens(c)
-    load("first", (out_first, wfirst))
-    load_w(1)
-    load("last", (out_last, wlast))
-
     barrier = pltpu.get_barrier_semaphore()
     for other in (left, right, far, partner):
         pl.semaphore_signal(barrier, inc=1, device_id=other, device_id_type=MESH)
@@ -203,13 +199,10 @@
             lhs[:, pl.ds(n * step, step)] = (x * gain_row(0, n, step)).astype(BF)
         project_qkv(0, c, jnp.sum(total, axis=1, keepdims=True))
 
-    def attended_rows(layer, c):
-        return jnp.concatenate([att[layer, t, chunk_rows(c), :] for t in range(tp_n)], axis=1)
-
     @scoped
     def trans(c, between=None):
         step = 256
-        a = attended_rows(0, c)
+        a = jnp.concatenate([att[0, t, chunk_rows(c), :] for t in range(tp_n)], axis=1)
         total = jnp.zeros((CHUNK, 128), F32)
         for n in range(width // step):
             part = pl.ds(n * step, step)
@@ -226,11 +219,12 @@
         project_qkv(1, c, jnp.sum(total, axis=1, keepdims=True))
 
     @scoped
-    def final(c):
-        a = attended_rows(1, c)
+    def final(c, count=1):
+        mine = pl.ds(c * CHUNK, count * CHUNK)
+        a = jnp.concatenate([att[1, t, mine, :] for t in range(tp_n)], axis=1)
         update = jnp.dot(a, wlast[...], preferred_element_type=F32)
-        own = h[chunk_rows(c), pl.ds(pl.multiple_of(me * cols, cols), cols)].astype(F32)
-        mixed[chunk_rows(c), :] = (own + update).astype(BF)
+        own = h[mine, pl.ds(pl.multiple_of(me * cols, cols), cols)].astype(F32)
+        mixed[mine, :] = (own + update).astype(BF)
 
     def scores_of(layer, p):
         window = pl.ds(PAIR * p, WIN)
@@ -350,10 +344,10 @@
         return layer == 0 or p in DIRECT
 
     def send_own(layer, p):
+        if is_direct(layer, p):
+            send(layer, p, me, far, far_sem(layer, p))
         send(layer, p, me, right, near_sem(layer, p))
         send(layer, p, me, left, near_sem(layer, p))
-        if is_direct(layer, p):
-            send(layer, p, me, far, far_sem(layer, p))
         send(layer, p, me, partner, partner_sem(layer, p))
 
     @scoped
@@ -398,6 +392,11 @@
     c3, c2, c1, c0 = order
     loads[("t", c3)].wait()
     dense(c3)
+    load("first", (out_first, wfirst))
+    load_w(1)
+    load("last", (out_last, wlast))
+    loads[("t", c2)].wait()
+    dense(c2)
     with jax.named_scope("barrier"):
         pl.semaphore_wait(barrier, 4 + jnp.where(sp > 0, 1, 0) + jnp.where(sp < sp_n - 1, 1, 0))
     send_halo(0, c3)
@@ -406,8 +405,6 @@
     def _():
         doc_halo().start()
 
-    loads[("t", c2)].wait()
-    dense(c2)
     send_halo(0, c2)
     loads[("t", c1)].wait()
     dense(c1)
@@ -422,61 +419,54 @@
 
     build_halo_docs()
     wait_halo(0, c3)
-    attend_send(0, 3, 2)
+    attend(0, 3, 2)
+    near(0, 7, 6)
+    distant(0, 7, 6)
+    send_own(0, 3)
+    send_own(0, 2)
     build_bias(1)
     loads["first"].wait()
     loads[("w", 1)].wait()
     loads["last"].wait()
-    near(0, 7, 6)
     wait_halo(0, c2)
     attend_send(0, 1, 0)
-    distant(0, 7, 6)
-    near(0, 5, 4)
     consume(0, c3)
 
-    def serve_0():
-        distant(0, 5, 4)
-        near(0, 3)
-
-    def serve_1():
-        near(0, 2)
-        distant(0, 3, 2)
-
-    def serve_2():
-        near(0, 1, 0)
-        distant(0, 1, 0)
-
-    trans(c3, between=serve_0)
+    def serve(*which):
+        near(0, *which)
+        distant(0, *which)
+
+    trans(c3, between=functools.partial(serve, 5, 4))
     send_halo(1, c3)
     consume(0, c2)
-    trans(c2, between=serve_1)
+    trans(c2, between=functools.partial(serve, 3, 2))
     send_halo(1, c2)
     consume(0, c1)
-    trans(c1, between=serve_2)
+    trans(c1)
+    serve(1, 0)
     attend_send(1, 7, 6)
     consume(0, c0)
     trans(c0)
     attend_send(1, 5, 4)
-    near(1, 7, 6)
     wait_halo(1, c3)
     attend_send(1, 3, 2)
-    distant(1, 7, 6)
     wait_halo(1, c2)
     attend_send(1, 1, 0)
+    near(1, 7, 6)
+    distant(1, 7, 6)
     near(1, 5, 4)
+    near(1, 3, 2)
     consume(1, c3)
     final(c3)
-    near(1, 3, 2)
-    distant(1, 5, 4)
     near(1, 1, 0)
-    distant(1, 3, 2)
-    consume(1, c2)
-    final(c2)
-    consume(1, c1)
-    final(c1)
     distant(1, 1, 0)
     consume(1, c0)
     final(c0)
+    distant(1, 5, 4)
+    distant(1, 3, 2)
+    consume(1, c2)
+    consume(1, c1)
+    final(c1, 2)
     with jax.named_scope("sends"):
         for layer in range(LAYERS):
             whole, rest = divmod(sent[layer], rows)
@@ -536,18 +526,23 @@
                 pltpu.SemaphoreType.DMA((LAYERS * (rows // CHUNK),)),
             ],
             compiler_params=pltpu.CompilerParams(
-                collective_id=0, has_side_effects=True, vmem_limit_bytes=60 * 1024 * 1024
+                collective_id=0, has_side_effects=True, vmem_limit_bytes=40 * 1024 * 1024
             ),
         )(
-            tokens,
-            doc_ids.reshape(rows // 128, 128),
-            gains,
-            w_query,
-            w_key,
-            w_value,
-            rel_table,
-            out_first,
-            out_last,
+            *[
+                pltpu.with_memory_space_constraint(x, pltpu.HBM)
+                for x in (
+                    tokens,
+                    doc_ids.reshape(rows // 128, 128),
+                    gains,
+                    w_query,
+                    w_key,
+                    w_value,
+                    rel_table,
+                    out_first,
+                    out_last,
+                )
+            ],
         )
 
     placed = (

time: 61.8 us -> 55.9 us (0.905)
  Pallas kernels: 59.8 us -> 55 us
  local copies, waits for them, and re-layouts: 1.87 us -> 0.8 us
    pallas_call x1, Pallas kernels: 59.8 us -> 55 us  [shards(): pl.pallas_call(functools.partial(kernel, sp_n, tp_n), out_shape=jax.Shape...]
    unnamed x1, local copies, waits for them, and re-layouts: 1.87 us -> 0.8 us
where the time goes in v2:
time: 55.9 us; the launch traced here: 55.8 us
  Pallas kernels  55 us (98%)
  local copies, waits for them, and re-layouts  0.8 us (1%)
    pallas_call x1, Pallas kernels, shards(): pl.pallas_call(functools.partial(kernel, sp_n, tp_n), out_shape=jax.Shape...  55 us

profile of v2, /device:TPU:33, one launch (start us, length us, event | category | flops | bytes accessed | tf_op | source)
XLA Modules:
  0.0 55.8 jit_solution(2997401817871947297)
XLA Ops:
  0.0 55.0 %shard_map.91 = bf16[1024,256]{1,0:T(8,128)(2,1)S(1)} custom-call(bf16[1024,2048]{1,0:T(8,128)(2,1)} %tokens.1, s32[8,128]{1,0:T(8,128)} %bitcast.1, bf16[2,2048]{1,0:T(2,128)(2,1)} %gains_in.1, bf16[2,2048,128]{2,1,0:T(8,128)(2,1)} %w_query.1, bf16[2,2048,128]{2,1,0:T(8,128)(2,1)} %w_key.1, bf16[2,2048,128]{2,1,0:T(8,128)(2,1)} %w_value.1, ...), custom_call_target="tpu_custom_call" | custom-call | tf_op jit(solution)/shard_map/pallas_call | solution.py:498
  55.0 0.8 %copy.11 = bf16[1024,256]{1,0:T(8,128)(2,1)} copy(bf16[1024,256]{1,0:T(8,128)(2,1)S(1)} %shard_map.91) | data formatting | bytes 1048576

commit v3 on v2

--- a/solution.py
+++ b/solution.py
@@ -18,7 +18,7 @@
 WIN = REACH + PAIR
 CHUNK = 2 * PAIR
 BIG = 1e30
-DIRECT = (7, 6, 1, 0)
+DIRECT = (3, 0)
 LOG2E = math.log2(math.e)
 MESH = pl.DeviceIdType.MESH
 BF = jnp.bfloat16
@@ -73,7 +73,6 @@
 ):
     rows, width = h.shape
     cols = wlast.shape[1]
-    pairs = rows // PAIR
     chunks = rows // CHUNK
     tail = REACH // CHUNK
     sp = lax.axis_index("sp")
@@ -119,8 +118,7 @@
     load("table", (table_in, table))
     load_tokens(order[0])
     load_w(0)
-    for c in order[1:]:
-        load_tokens(c)
+    load_tokens(order[1])
     barrier = pltpu.get_barrier_semaphore()
     for other in (left, right, far, partner):
         pl.semaphore_signal(barrier, inc=1, device_id=other, device_id_type=MESH)
@@ -320,60 +318,57 @@
 
     sent = [0] * LAYERS
 
-    def send(layer, p, slot, device, recv_sem, part=None):
-        first = PAIR * p + (SEG if part == 1 else 0)
-        count = PAIR if part is None else SEG
+    def send(layer, c, slot, device, recv_sem, part=None):
+        first = CHUNK * c + (PAIR if part == 1 else 0)
+        count = CHUNK if part is None else PAIR
         ref = att.at[layer, slot, pl.ds(first, count)]
         remote(ref, ref, ag_send.at[layer], recv_sem, device).start()
         sent[layer] += count
 
-    def arrived(layer, slots, count, recv_sem):
-        ref = att.at[layer, 0:slots, pl.ds(0, count)]
+    def arrived(layer, slots, recv_sem):
+        ref = att.at[layer, 0:slots, pl.ds(0, CHUNK)]
         remote(ref, ref, ag_send.at[layer], recv_sem, partner).wait_recv()
 
-    def near_sem(layer, p):
-        return near_recv.at[layer * pairs + p]
-
-    def far_sem(layer, p):
-        return far_recv.at[layer * pairs + p]
-
-    def partner_sem(layer, p):
-        return partner_recv.at[layer * chunks + p // 2]
-
-    def is_direct(layer, p):
-        return layer == 0 or p in DIRECT
-
-    def send_own(layer, p):
-        if is_direct(layer, p):
-            send(layer, p, me, far, far_sem(layer, p))
-        send(layer, p, me, right, near_sem(layer, p))
-        send(layer, p, me, left, near_sem(layer, p))
-        send(layer, p, me, partner, partner_sem(layer, p))
-
-    @scoped
-    def near(layer, *which):
-        for p in which:
-            arrived(layer, 2, PAIR, near_sem(layer, p))
-            if not is_direct(layer, p):
-                send(layer, p, left_i, right, far_sem(layer, p), 0)
-                send(layer, p, right_i, left, far_sem(layer, p), 1)
-            send(layer, p, left_i, partner, partner_sem(layer, p))
-            send(layer, p, right_i, partner, partner_sem(layer, p))
-
-    @scoped
-    def distant(layer, *which):
-        for p in which:
-            arrived(layer, 1, PAIR, far_sem(layer, p))
-            send(layer, p, far_i, partner, partner_sem(layer, p))
+    def near_sem(layer, c):
+        return near_recv.at[layer * chunks + c]
+
+    def far_sem(layer, c):
+        return far_recv.at[layer * chunks + c]
+
+    def partner_sem(layer, c):
+        return partner_recv.at[layer * chunks + c]
+
+    def is_direct(layer, c):
+        return layer == 0 or c in DIRECT
+
+    def send_own(layer, c):
+        if is_direct(layer, c):
+            send(layer, c, me, far, far_sem(layer, c))
+        send(layer, c, me, right, near_sem(layer, c))
+        send(layer, c, me, left, near_sem(layer, c))
+        send(layer, c, me, partner, partner_sem(layer, c))
+
+    @scoped
+    def near(layer, c):
+        arrived(layer, 2, near_sem(layer, c))
+        if not is_direct(layer, c):
+            send(layer, c, left_i, right, far_sem(layer, c), 0)
+            send(layer, c, right_i, left, far_sem(layer, c), 1)
+        send(layer, c, left_i, partner, partner_sem(layer, c))
+        send(layer, c, right_i, partner, partner_sem(layer, c))
+
+    @scoped
+    def distant(layer, c):
+        arrived(layer, 1, far_sem(layer, c))
+        send(layer, c, far_i, partner, partner_sem(layer, c))
 
     @scoped
     def consume(layer, c):
-        arrived(layer, tp_n, PAIR, partner_sem(layer, 2 * c))
-
-    def attend_send(layer, *which):
-        attend(layer, *which)
-        for p in which:
-            send_own(layer, p)
+        arrived(layer, tp_n // 2, partner_sem(layer, c))
+
+    def attend_send(layer, c):
+        attend(layer, 2 * c + 1, 2 * c)
+        send_own(layer, c)
 
     @pl.when(sp == 0)
     def _():
@@ -387,6 +382,8 @@
     build_docs()
     loads["table"].wait()
     build_bias(0)
+    for c in order[2:]:
+        load_tokens(c)
     loads["gains"].wait()
     loads[("w", 0)].wait()
     c3, c2, c1, c0 = order
@@ -408,10 +405,10 @@
     send_halo(0, c2)
     loads[("t", c1)].wait()
     dense(c1)
-    attend_send(0, 7, 6)
+    attend_send(0, c3)
     loads[("t", c0)].wait()
     dense(c0)
-    attend_send(0, 5, 4)
+    attend_send(0, c2)
 
     @pl.when(sp > 0)
     def _():
@@ -420,50 +417,49 @@
     build_halo_docs()
     wait_halo(0, c3)
     attend(0, 3, 2)
-    near(0, 7, 6)
-    distant(0, 7, 6)
-    send_own(0, 3)
-    send_own(0, 2)
+    near(0, c3)
+    distant(0, c3)
+    send_own(0, c1)
     build_bias(1)
     loads["first"].wait()
     loads[("w", 1)].wait()
     loads["last"].wait()
     wait_halo(0, c2)
-    attend_send(0, 1, 0)
+    attend_send(0, c0)
     consume(0, c3)
 
-    def serve(*which):
-        near(0, *which)
-        distant(0, *which)
-
-    trans(c3, between=functools.partial(serve, 5, 4))
+    def serve(c):
+        near(0, c)
+        distant(0, c)
+
+    trans(c3, between=functools.partial(serve, c2))
     send_halo(1, c3)
     consume(0, c2)
-    trans(c2, between=functools.partial(serve, 3, 2))
+    trans(c2, between=functools.partial(serve, c1))
     send_halo(1, c2)
     consume(0, c1)
     trans(c1)
-    serve(1, 0)
-    attend_send(1, 7, 6)
+    serve(c0)
+    attend_send(1, c3)
     consume(0, c0)
     trans(c0)
-    attend_send(1, 5, 4)
+    attend_send(1, c2)
     wait_halo(1, c3)
-    attend_send(1, 3, 2)
+    attend_send(1, c1)
     wait_halo(1, c2)
-    attend_send(1, 1, 0)
-    near(1, 7, 6)
-    distant(1, 7, 6)
-    near(1, 5, 4)
-    near(1, 3, 2)
+    attend_send(1, c0)
+    near(1, c3)
+    distant(1, c3)
+    near(1, c2)
+    near(1, c1)
     consume(1, c3)
     final(c3)
-    near(1, 1, 0)
-    distant(1, 1, 0)
+    near(1, c0)
+    distant(1, c0)
     consume(1, c0)
     final(c0)
-    distant(1, 5, 4)
-    distant(1, 3, 2)
+    distant(1, c2)
+    distant(1, c1)
     consume(1, c2)
     consume(1, c1)
     final(c1, 2)
@@ -521,8 +517,8 @@
                 pltpu.SemaphoreType.DMA((halos,)),
                 pltpu.SemaphoreType.DMA((halos,)),
                 pltpu.SemaphoreType.DMA((LAYERS,)),
-                pltpu.SemaphoreType.DMA((LAYERS * (rows // PAIR),)),
-                pltpu.SemaphoreType.DMA((LAYERS * (rows // PAIR),)),
+                pltpu.SemaphoreType.DMA((LAYERS * (rows // CHUNK),)),
+                pltpu.SemaphoreType.DMA((LAYERS * (rows // CHUNK),)),
                 pltpu.SemaphoreType.DMA((LAYERS * (rows // CHUNK),)),
             ],
             compiler_params=pltpu.CompilerParams(

time: 55.9 us -> 55.6 us (level)
  no operation moved by 1% of the time
where the time goes in v3:
time: 55.6 us; the launch traced here: 55.5 us
  Pallas kernels  54.7 us (98%)
  local copies, waits for them, and re-layouts  0.8 us (1%)
    pallas_call x1, Pallas kernels, shards(): pl.pallas_call(functools.partial(kernel, sp_n, tp_n), out_shape=jax.Shape...  54.7 us

profile of v3, /device:TPU:33, one launch (start us, length us, event | category | flops | bytes accessed | tf_op | source)
XLA Modules:
  0.0 55.5 jit_solution(12755127065533583188)
XLA Ops:
  0.0 54.7 %shard_map.91 = bf16[1024,256]{1,0:T(8,128)(2,1)S(1)} custom-call(bf16[1024,2048]{1,0:T(8,128)(2,1)} %tokens.1, s32[8,128]{1,0:T(8,128)} %bitcast.1, bf16[2,2048]{1,0:T(2,128)(2,1)} %gains_in.1, bf16[2,2048,128]{2,1,0:T(8,128)(2,1)} %w_query.1, bf16[2,2048,128]{2,1,0:T(8,128)(2,1)} %w_key.1, bf16[2,2048,128]{2,1,0:T(8,128)(2,1)} %w_value.1, ...), custom_call_target="tpu_custom_call" | custom-call | tf_op jit(solution)/shard_map/pallas_call | solution.py:494
  54.7 0.8 %copy.11 = bf16[1024,256]{1,0:T(8,128)(2,1)} copy(bf16[1024,256]{1,0:T(8,128)(2,1)S(1)} %shard_map.91) | data formatting | bytes 1048576
